TPU v7x, 32 devices: a whole 2x2x4 slice. The times are simulated.
32 devices in a mesh: sp: 8 (over z, x), tp: 4 (over y, core).
Axes of the slice: x: 2, y: 2, z: 4, core: 2. Of those that a mesh axis runs over, the one named last changes fastest.
Arguments:
- residual: bfloat16 [2048, 2048], P('sp', 'tp'), may hold values from -48 to 48
- queries: bfloat16 [2048, 1024], P('sp', 'tp'), may hold values from -6 to 6
- key_rows: bfloat16 [2048, 512], P('sp', 'tp'), may hold values from -6 to 6
- value_rows: bfloat16 [2048, 512], P('sp', 'tp'), may hold values from -6 to 6
- break_shift: bfloat16 [4, 2048], P('tp', 'sp'), may hold values from -20 to 0
- head_gain: float32 [1024], P('tp'), may hold values from 0.1 to 1.9
- out_weight: bfloat16 [1024, 2048], P('tp'), may hold values from -0.1875 to 0.1875
- mlp_gain: float32 [2048], replicated, may hold values from 0.1 to 1.9
- up_weight: bfloat16 [2048, 8192], P('sp', 'tp'), may hold values from -0.125 to 0.125
- down_weight: bfloat16 [8192, 2048], P('tp', 'sp'), may hold values from -0.0625 to 0.0625
Outputs:
- layer_out: bfloat16 [2048, 2048], P('sp', 'tp')
All inputs are finite; a program needn't handle non-finite values.
Results may differ from a plain program's by a relative error of at most 0.013.
Values may be sent and summed in bfloat16 or wider, within the bound.
A program may use at most 128 MiB of HBM per device.

v0:
```python
import jax
import jax.numpy as jnp
from jax import lax
from jax.sharding import PartitionSpec as P

HEAD_DIM = 128


eps = 1e-06


def stick_attention(queries, key_all, value_all, shift_all, first_pos, key_block):
    token_count = queries.shape[0]
    kv_local = key_all.shape[1] // HEAD_DIM
    query_local = queries.shape[1] // HEAD_DIM
    group_size = query_local // kv_local
    stacked = queries.reshape(token_count, kv_local, group_size, HEAD_DIM).transpose(1, 2, 0, 3)
    stacked = stacked.reshape(kv_local, group_size * token_count, HEAD_DIM)
    query_pos = first_pos + lax.iota(jnp.int32, group_size * token_count) % token_count
    score_scale = HEAD_DIM ** (-0.5)
    block_count = (first_pos + token_count - 1 + key_block - 1) // key_block

    def one_block(turn_index, state_pair):
        running, broken_after = state_pair
        offset = (block_count - 1 - turn_index) * key_block
        key_block_rows = lax.dynamic_slice_in_dim(key_all, offset, key_block, 0).reshape(
            key_block, kv_local, HEAD_DIM
        )
        value_block_rows = lax.dynamic_slice_in_dim(value_all, offset, key_block, 0).reshape(
            key_block, kv_local, HEAD_DIM
        )
        shift_block = lax.dynamic_slice_in_dim(shift_all, offset, key_block, 1).astype(jnp.float32)
        scores = jnp.einsum(
            "grd,kgd->grk", stacked, key_block_rows, preferred_element_type=jnp.float32
        )
        scores = scores * score_scale + shift_block[:, None, :]
        key_pos = offset + lax.iota(jnp.int32, key_block)
        visible = key_pos[None, None, :] < query_pos[None, :, None]
        broken = jnp.where(visible, jax.nn.log_sigmoid(-scores), 0.0)
        later = lax.cumsum(broken, axis=2, reverse=True) - broken + broken_after[:, :, None]
        weights = jnp.where(visible, jnp.exp(jax.nn.log_sigmoid(scores) + later), 0.0).astype(
            jnp.bfloat16
        )
        running = running + jnp.einsum(
            "grk,kgd->grd", weights, value_block_rows, preferred_element_type=jnp.float32
        )
        return (running, broken_after + jnp.sum(broken, axis=2))

    start_pair = (
        jnp.zeros((kv_local, group_size * token_count, HEAD_DIM), jnp.float32),
        jnp.zeros((kv_local, group_size * token_count), jnp.float32),
    )
    running, broken_after = lax.fori_loop(0, block_count, one_block, start_pair)
    running = running.reshape(kv_local, group_size, token_count, HEAD_DIM).transpose(2, 0, 1, 3)
    return running.reshape(token_count, query_local, HEAD_DIM)


def body(
    residual,
    queries,
    key_rows,
    value_rows,
    break_shift,
    head_gain,
    out_weight,
    mlp_gain,
    up_weight,
    down_weight,
):
    token_count = queries.shape[0]
    first_pos = lax.axis_index("sp") * token_count
    key_all, value_all, shift_all = (
        lax.all_gather(key_rows, "sp", axis=0, tiled=True),
        lax.all_gather(value_rows, "sp", axis=0, tiled=True),
        lax.all_gather(break_shift, "sp", axis=1, tiled=True),
    )
    key_block = min(2048, key_all.shape[0])
    mixed = stick_attention(queries, key_all, value_all, shift_all, first_pos, key_block)
    power = jnp.mean(mixed * mixed, axis=2, keepdims=True)
    attended = (mixed * lax.rsqrt(power + eps) * head_gain.reshape(-1, HEAD_DIM)).astype(
        jnp.bfloat16
    )
    attended = attended.reshape(token_count, -1)
    partial_value = jnp.dot(attended, out_weight, preferred_element_type=jnp.float32)
    column_count = residual.shape[1]
    column_start = lax.axis_index("tp") * column_count
    own_part = lax.dynamic_slice_in_dim(
        partial_value, column_start, column_count, 1
    ) + residual.astype(jnp.float32)
    partial_value = lax.dynamic_update_slice_in_dim(partial_value, own_part, column_start, 1)
    hidden_whole = lax.psum(partial_value, "tp").astype(jnp.bfloat16)
    widened = hidden_whole.astype(jnp.float32)
    inverse = lax.rsqrt(jnp.mean(widened * widened, axis=1, keepdims=True) + eps)
    mlp_in = (widened * inverse * mlp_gain).astype(jnp.bfloat16)
    hidden_state = lax.dynamic_slice_in_dim(hidden_whole, column_start, column_count, 1)
    lifted = jnp.dot(
        mlp_in,
        lax.all_gather(up_weight, "sp", axis=0, tiled=True),
        preferred_element_type=jnp.float32,
    )
    activated = jnp.square(jax.nn.relu(lifted)).astype(jnp.bfloat16)
    expanded = jnp.dot(
        activated,
        lax.all_gather(down_weight, "sp", axis=1, tiled=True),
        preferred_element_type=jnp.float32,
    )
    mlp_total = lax.psum_scatter(
        expanded.astype(jnp.bfloat16), "tp", scatter_dimension=1, tiled=True
    ).astype(jnp.float32)
    return (hidden_state.astype(jnp.float32) + mlp_total).astype(jnp.bfloat16)


def solution(mesh):
    in_specs = (
        P("sp", "tp"),
        P("sp", "tp"),
        P("sp", "tp"),
        P("sp", "tp"),
        P("tp", "sp"),
        P("tp"),
        P("tp", None),
        P(),
        P("sp", "tp"),
        P("tp", "sp"),
    )
    out_specs = P("sp", "tp")
    return jax.shard_map(body, mesh=mesh, in_specs=in_specs, out_specs=out_specs, check_vma=False)
```

profile of v0, /device:TPU:8, one launch (start us, length us, event | category | flops | bytes accessed | tf_op | source)
XLA Modules:
  0.0 311.0 jit_solution(17928566602720874883)
XLA Ops:
  6.5 0.0 copy-start
  6.5 0.0 all-gather.3.cloned.1.call-start
  6.5 0.7 all-gather.3.cloned.1.call-update
  7.3 0.0 all-gather.5.cloned.1.call-start
  7.3 0.7 all-gather.5.cloned.1.call-update
  8.0 0.0 reduce-scatter.2.cloned.1.call-start
  8.1 31.3 %all_gather.15 = bf16[2048,128]{1,0:T(8,128)(2,1)S(1)} all-gather(bf16[256,128]{1,0:T(8,128)(2,1)} %param.14), channel_id=1, replica_groups=mesh['sp'=8,'tp'=4] {'sp'}, dimensions={0}, use_global_device_ids=true | all-gather | bytes 589824 | tf_op jit(solution)/shard_map/all_gather | solution.py:73
  39.3 33.3 %all_gather.17 = bf16[2048,128]{1,0:T(8,128)(2,1)S(1)} all-gather(bf16[256,128]{1,0:T(8,128)(2,1)} %param.15), channel_id=1, replica_groups=mesh['sp'=8,'tp'=4] {'sp'}, dimensions={0}, use_global_device_ids=true | all-gather | bytes 589824 | tf_op jit(solution)/shard_map/all_gather | solution.py:74
  72.7 0.9 reshape.144
  73.6 21.8 %all_gather.16 = bf16[1,2048]{1,0:T(2,128)(2,1)S(1)} all-gather(bf16[1,256]{1,0:T(2,128)(2,1)} %param.16), channel_id=1, replica_groups=mesh['sp'=8,'tp'=4] {'sp'}, dimensions={1}, use_global_device_ids=true | all-gather | bytes 4608 | tf_op jit(solution)/shard_map/all_gather | solution.py:75
  95.5 0.0 copy-start.3
  95.5 48.3 %while.15 = (s32[]{:T(128)}, f32[1,512,128]{2,1,0:T(8,128)S(1)}, f32[1,512]{1,0:T(1,128)S(1)}, s32[]{:T(128)}, s32[]{:T(128)}, /*index=5*/bf16[1,512,128]{2,1,0:...) while((s32[]{:T(128)}, f32[1,512,128]{2,1,0:T(8,128)S(1)}, ...), condition=%wide.region_4.5_spmd.clone, body=%wide.region_0.4_spmd.clone.sunk | while | flops 709041152 | bytes 81762496 | solution.py:53
  95.5 2.6 fusion.64
  98.2 5.0 %fusion.66 = (f32[512]{0:T(512)S(1)}, f32[64,8,16,128]{3,1,2,0:T(8,128)S(1)}) fusion(f32[2048]{0:T(1024)S(1)} %bitcast.98, f32[512,2048]{1,0:T(8,128)} %fusion.64, s32[512]{0:T(512)S(1)} %fusion.65, s32[2048]{0:T(1024)S(1)} %iota_add_fusion.2), kind=kLoop, calls=%fused_computation.30.clone.1 | loop fusion | flops 12582400 | bytes 8409088 | tf_op jit(solution)/shard_map/while/body/reduce_sum | solution.py:47
  103.2 2.9 copy.47
  106.1 5.6 %copy.48 = f32[1,512,16,128]{1,2,3,0:T(8,128)} copy(f32[1,512,16,128]{3,2,1,0:T(8,128)} %bitcast.92) | data formatting | bytes 8388608 | tf_op jit(solution)/shard_map/reshape.112
  111.7 10.8 %fusion.67 = f32[1,512,16,128]{1,2,3,0:T(8,128)S(1)} fusion(f32[1,512,16,128]{1,2,3,0:T(8,128)} %copy.48), kind=kOutput, calls=%fused_computation.52.clone.1 | output fusion | flops 133169152 | bytes 8388608 | tf_op jit(solution)/shard_map/reduce-window.4
  122.5 0.0 copy-start.1
  122.5 1.9 copy-done.1
  124.5 0.1 reduce-window.20
  124.6 0.1 copy.49
  124.7 2.6 broadcast.100
  127.3 5.8 %copy.50 = f32[1,512,16,128]{3,2,1,0:T(8,128)} copy(f32[1,512,16,128]{1,2,3,0:T(8,128)} %copy-done.1) | data formatting | bytes 8388608 | tf_op jit(solution)/shard_map/reduce-window.4
  133.1 10.4 %fusion.68 = f32[1,512,128]{2,1,0:T(8,128)S(1)} fusion(f32[1,512,128]{2,1,0:T(8,128)S(1)} %get-tuple-element.245, bf16[2048,128]{1,0:T(8,128)(2,1)S(1)} %get-tuple-element.265, f32[64,8,16,128]{3,2,1,0:T(8,128)} %bitcast.93, f32[64,8,16,128]{3,2,1,0:T(8,128)} %bitcast.94, f32[512,2048]{1,0:T(8,128)} %fusion.64, f32[512]{0:T(512)S(1)} %bitcast.101, ...), kind=kOutput, calls=%fused_computation.16.clone.1 | convolution fusion | flops 294715392 | bytes 13651968 | tf_op jit(solution)/shard_map/while/body/grk,kgd->grd/dot_general | solution.py:44
  143.7 0.0 copy-start.2
  143.8 0.1 copy.23
  143.9 0.1 multiply_reduce_fusion
  144.1 0.0 copy-done.3
  144.1 0.1 fusion.38
  144.2 0.0 copy-done
  144.2 0.0 copy-start.4
  144.2 0.5 fusion.41
  144.7 0.0 copy-done.2
  144.7 0.1 add_dynamic-update-slice_fusion
  144.8 40.5 %all-reduce.1 = bf16[256,2048]{1,0:T(8,128)(2,1)} all-reduce(f32[256,2048]{1,0:T(8,128)S(1)} %add_dynamic-update-slice_fusion), channel_id=1, replica_groups=mesh['sp'=8,'tp'=4] {'tp'}, use_global_device_ids=true, to_apply=%region_6.7 | all-reduce | flops 524288 | bytes 3145728 | tf_op jit(solution)/shard_map/psum | solution.py:91
  185.3 1.5 fusion.29
  186.8 0.0 all-gather.3.cloned.1.call-done
  186.8 79.2 %all-gather.5.cloned.1.call-done = bf16[2048,2048]{1,0:T(8,128)(2,1)} async-done(((bf16[2048,256]{1,0:T(8,128)(2,1)}), bf16[2048,2048]{1,0:T(8,128)(2,1)}) %all-gather.5.cloned.1.call-update) | async-done | bytes 8388624 | tf_op jit(solution)/shard_map/all_gather | solution.py:104
  266.0 0.0 copy-done.4
  266.0 11.6 %convolution_convert_fusion = bf16[256,2048]{1,0:T(8,128)(2,1)} fusion(bf16[2048,2048]{1,0:T(8,128)(2,1)} %all-gather.5.cloned.1.call-done, bf16[2048,2048]{1,0:T(8,128)(2,1)} %all-gather.3.cloned.1.call-done, bf16[256,2048]{1,0:T(8,128)(2,1)} %all-reduce.1, f32[2048]{0:T(1024)S(1)} %copy-done.4, f32[256]{0:T(256)S(1)} %add_rsqrt_fusion.1), kind=kOutput, calls=%fused_computation.37 | convolution fusion | flops 4299161600 | bytes 18883584 | tf_op jit(solution)/shard_map/dot_general | solution.py:102
  277.7 0.0 reduce-scatter.2.cloned.1.call-update
  277.7 25.0 %reduce-scatter.2.cloned.1.call-done = bf16[256,512]{1,0:T(8,128)(2,1)} async-done(((bf16[256,2048]{1,0:T(8,128)(2,1)}), bf16[256,512]{1,0:T(8,128)(2,1)}) %reduce-scatter.2.cloned.1.call-update) | async-done | bytes 262160 | tf_op jit(solution)/shard_map/reduce_scatter | solution.py:107
  302.6 1.8 add_convert_fusion
  (11 shorter events, 0.1 us)
Async XLA Ops:
  6.5 137.6 %copy-start = (bf16[256,2048]{1,0:T(8,128)(2,1)S(1)}, bf16[256,2048]{1,0:T(8,128)(2,1)}, u32[]{:S(2)}) copy-start(bf16[256,2048]{1,0:T(8,128)(2,1)} %param.18) | copy-start | bytes 3145732
  6.5 180.3 %all-gather.3.cloned.1.call-start = ((), (), s32[]{:S(2)}) async-start(), calls=%async_computation.1 | async-start | bytes 9437184 | tf_op jit(solution)/shard_map/all_gather | solution.py:98
  7.3 258.7 %all-gather.5.cloned.1.call-start = ((), (), s32[]{:S(2)}) async-start(), calls=%async_computation.2 | async-start | bytes 9437184 | tf_op jit(solution)/shard_map/all_gather | solution.py:104
  8.0 294.6 %reduce-scatter.2.cloned.1.call-start = ((), (), s32[]{:S(2)}) async-start(), calls=%async_computation.3 | async-start | bytes 1310720 | tf_op jit(solution)/shard_map/reduce_scatter | solution.py:107
  95.5 48.6 %copy-start.3 = (f32[256]{0:T(256)S(1)}, f32[256]{0:T(256)}, u32[]{:S(2)}) copy-start(f32[256]{0:T(256)} %param.17) | copy-start | bytes 3076
  122.5 1.9 copy-start.1
  143.7 1.0 copy-start.2
  144.2 121.8 %copy-start.4 = (f32[2048]{0:T(1024)S(1)}, f32[2048]{0:T(1024)}, u32[]{:S(2)}) copy-start(f32[2048]{0:T(1024)} %param.19) | copy-start | bytes 24580
Sparse Core Ops, SparseCore 0:
  9.5 131.8 all-gather.2
  143.4 122.5 all-gather.4
  277.8 24.8 reduce-scatter.1
where the time goes:
time: 313 us; the launch traced here: 311 us
  blocking collectives  127 us (41%)
  waiting for transfers between devices  106 us (34%)
  matrix products  25.2 us (8%)
  local copies, waits for them, and re-layouts  20.2 us (6%)
  other arithmetic  19.6 us (6%)
  between operations  13.2 us (4%)
    all_gather x1, waiting for transfers between devices, body(): lax.all_gather(down_weight, 'sp', axis=1, tiled=True)  79.2 us
    psum x1, blocking collectives, body(): hidden_whole = lax.psum(partial_value, 'tp').astype(jnp.bfloat16)  40.5 us
    all_gather x1, blocking collectives, body(): lax.all_gather(value_rows, 'sp', axis=0, tiled=True)  33.3 us
    all_gather x1, blocking collectives, body(): lax.all_gather(key_rows, 'sp', axis=0, tiled=True)  31.3 us
    reduce_scatter x1, waiting for transfers between devices, body(): lax.psum_scatter(expanded.astype(jnp.bfloat16), 'tp', scatter_dimension=1...  25 us
    all_gather x1, blocking collectives, body(): lax.all_gather(break_shift, 'sp', axis=1, tiled=True)  21.8 us
    another operation x6, local copies, waits for them, and re-layouts  14.2 us
    dot_general x1, matrix products, body(): jnp.dot(activated, lax.all_gather(down_weight, 'sp', axis=1, tiled=True),...  11.6 us
  transfers between devices with their start and end apart: 3, of which 2 were waited for; matrix products, arithmetic and copies ran while one was open for 16% of the time, Pallas kernels for 0%

commit v1 on v0

--- a/solution.py
+++ b/solution.py
@@ -1,6 +1,10 @@
+import functools
+
 import jax
 import jax.numpy as jnp
 from jax import lax
+from jax.experimental import pallas as pl
+from jax.experimental.pallas import tpu as pltpu
 from jax.sharding import PartitionSpec as P
 
 HEAD_DIM = 128
@@ -55,7 +59,7 @@
     return running.reshape(token_count, query_local, HEAD_DIM)
 
 
-def body(
+def gathered_body(
     residual,
     queries,
     key_rows,
@@ -110,6 +114,477 @@
     return (hidden_state.astype(jnp.float32) + mlp_total).astype(jnp.bfloat16)
 
 
+PAIR = 2
+F32, BF16 = jnp.float32, jnp.bfloat16
+
+
+def sem_bases(depth, members):
+    names = (
+        ("kvz", depth), ("kvx", depth), ("shz", depth), ("shx", depth),
+        ("upz", depth), ("dnz", depth), ("upx", depth), ("dnx", depth),
+        ("res", members), ("hid", members), ("pc", PAIR), ("py", 1),
+        ("mz", depth), ("my", depth), ("mc", PAIR * depth),
+        ("rc", PAIR * depth), ("ry", depth), ("rz", depth),
+    )
+    base, total = {}, 0
+    for name, count in names:
+        base[name] = total
+        total += count
+    return base, total
+
+
+def layer_kernel(
+    depth, members, queries, keys, values, shift, gain, residual, out_weight, mlp_gain, up, down,
+    out, kv_all, shift_all, up_all, down_all, own_f32, own_cut, pair_part, y_cut, y_part,
+    res_all, hid_cut, hid_all, rows_all, share, pair_share, y_sum, y_share, z_sum, z_share,
+    own_total, send_sem, recv_sem, local_sem,
+):
+    base, _ = sem_bases(depth, members)
+    me, m = lax.axis_index("sp"), lax.axis_index("tp")
+    z, x, y, c = me // PAIR, me % PAIR, m // PAIR, m % PAIR
+    tokens = queries.shape[0]
+    row_part = tokens // members
+    sub = up_all.shape[1]
+    block = up.shape[0]
+    column_part = residual.shape[1]
+
+    def toward(e):
+        far = z
+        bit = 1
+        while bit < depth:
+            if e & bit:
+                far = far + bit - 2 * bit * ((z // bit) % 2)
+            bit *= 2
+        return far
+
+    def remote(src, dst, name, send, recv, sp=me, tp=m):
+        return pltpu.make_async_remote_copy(
+            src_ref=src, dst_ref=dst, send_sem=send_sem.at[base[name] + send],
+            recv_sem=recv_sem.at[base[name] + recv], device_id={"sp": sp, "tp": tp},
+            device_id_type=pl.DeviceIdType.MESH,
+        )
+
+    far_x, far_y, far_c = z * PAIR + 1 - x, (1 - y) * PAIR + c, y * PAIR + 1 - c
+
+    barrier = pltpu.get_barrier_semaphore()
+    peers = [(toward(e) * PAIR + x, m) for e in range(1, depth)] + [(far_x, m)]
+    peers += [(me, (m + d) % members) for d in range(1, members)]
+    for sp, tp in peers:
+        pl.semaphore_signal(
+            barrier, inc=1, device_id={"sp": sp, "tp": tp}, device_id_type=pl.DeviceIdType.MESH
+        )
+    first = [
+        pltpu.make_async_copy(keys, kv_all.at[me, 0], local_sem.at[0]),
+        pltpu.make_async_copy(values, kv_all.at[me, 1], local_sem.at[1]),
+        pltpu.make_async_copy(shift, shift_all.at[me], local_sem.at[2]),
+    ]
+
+    def up_piece(at):
+        return up.at[:, pl.ds(pl.multiple_of(at * sub, sub), sub)]
+
+    def down_piece(at):
+        return down.at[pl.ds(pl.multiple_of(at * sub, sub), sub), :]
+
+    def up_slot(at):
+        return up_all.at[pl.ds(pl.multiple_of(at * block, block), block), :]
+
+    def down_slot(zz, xx):
+        return down_all.at[zz, :, pl.ds(pl.multiple_of(xx * block, block), block)]
+
+    own_weights = [
+        pltpu.make_async_copy(up_piece(z), up_slot(me), local_sem.at[3]),
+        pltpu.make_async_copy(down_piece(z), down_slot(z, x), local_sem.at[4]),
+    ]
+    for copy in first + own_weights:
+        copy.start()
+    for copy in first:
+        copy.wait()
+    pl.semaphore_wait(barrier, len(peers))
+
+    def kv_z(far):
+        sp = far * PAIR + x
+        return (
+            remote(kv_all.at[me], kv_all.at[me], "kvz", far, z, sp=sp),
+            remote(shift_all.at[me], shift_all.at[me], "shz", far, z, sp=sp),
+        )
+
+    def kv_x(zz, xx):
+        at = zz * PAIR + xx
+        return (
+            remote(kv_all.at[at], kv_all.at[at], "kvx", zz, zz, sp=far_x),
+            remote(shift_all.at[at], shift_all.at[at], "shx", zz, zz, sp=far_x),
+        )
+
+    def kv_z_in(zz):
+        at = zz * PAIR + x
+        return (
+            remote(kv_all.at[at], kv_all.at[at], "kvz", zz, zz, sp=far_x),
+            remote(shift_all.at[at], shift_all.at[at], "shz", zz, zz, sp=far_x),
+        )
+
+    def weight_z(far):
+        sp = far * PAIR + x
+        return (
+            remote(up_piece(far), up_slot(me), "upz", far, z, sp=sp),
+            remote(down_piece(far), down_slot(z, x), "dnz", far, z, sp=sp),
+        )
+
+    def weight_x(zz, xx):
+        slot = up_slot(zz * PAIR + xx)
+        cell = down_slot(zz, xx)
+        return (
+            remote(slot, slot, "upx", zz, zz, sp=far_x),
+            remote(cell, cell, "dnx", zz, zz, sp=far_x),
+        )
+
+    def weight_z_in(zz):
+        slot = up_slot(zz * PAIR + x)
+        cell = down_slot(zz, x)
+        return (
+            remote(slot, slot, "upz", zz, zz, sp=far_x),
+            remote(cell, cell, "dnz", zz, zz, sp=far_x),
+        )
+
+    def start(copies):
+        for copy in copies:
+            copy.start()
+
+    def wait_send(copies):
+        for copy in copies:
+            copy.wait_send()
+
+    def wait_recv(copies):
+        for copy in copies:
+            copy.wait_recv()
+
+    def residual_out(far):
+        rows = pl.ds(pl.multiple_of(far * row_part, row_part), row_part)
+        return remote(residual.at[rows, :], res_all.at[m], "res", far, m, tp=far)
+
+    for d in range(1, depth):
+        @pl.when(z + d < depth)
+        def _():
+            start(kv_z(z + d))
+    start(kv_x(z, x))
+    for d in range(1, members):
+        residual_out((m + d) % members).start()
+    for d in range(1, depth):
+        @pl.when(z - d >= 0)
+        def _():
+            start(weight_z(z - d))
+    for copy in own_weights:
+        copy.wait()
+    start(weight_x(z, x))
+    for d in range(1, depth):
+        @pl.when(z + d < depth)
+        def _():
+            wait_send(kv_z(z + d))
+    for d in range(1, depth):
+        @pl.when(z + d < depth)
+        def _():
+            start(weight_z(z + d))
+
+    group = queries.shape[1] // HEAD_DIM
+    stacked = jnp.concatenate(
+        [queries[:, g * HEAD_DIM : (g + 1) * HEAD_DIM] for g in range(group)], axis=0
+    )
+    grid = (group * tokens, tokens)
+    lag = lax.broadcasted_iota(jnp.int32, grid, 1) - lax.broadcasted_iota(
+        jnp.int32, grid, 0
+    ) % tokens
+    square = (tokens, tokens)
+    later_keys = jnp.where(
+        lax.broadcasted_iota(jnp.int32, square, 0) > lax.broadcasted_iota(jnp.int32, square, 1),
+        1.0, 0.0,
+    ).astype(BF16)
+
+    def key_step(at, state):
+        running, after = state
+        scores = lax.dot_general(
+            stacked, kv_all[at, 0], (((1,), (1,)), ((), ())), preferred_element_type=F32
+        ) * (HEAD_DIM ** (-0.5)) + shift_all[at][0:1, :]
+        visible = lag < (me - at) * tokens
+        tail = jnp.log(1.0 + jnp.exp(-jnp.abs(scores)))
+        broken = jnp.where(visible, -(jnp.maximum(scores, 0.0) + tail), 0.0)
+        high = broken.astype(BF16)
+        low = (broken - high.astype(F32)).astype(BF16)
+        later = jnp.dot(high, later_keys, preferred_element_type=F32) + jnp.dot(
+            low, later_keys, preferred_element_type=F32
+        )
+        stick = jnp.where(
+            visible, jnp.exp(jnp.minimum(scores, 0.0) - tail + (later + after)), 0.0
+        ).astype(BF16)
+        running = running + jnp.dot(stick, kv_all[at, 1], preferred_element_type=F32)
+        return running, after + jnp.sum(broken, axis=1, keepdims=True)
+
+    def key_round(r, state):
+        zz = z - r
+
+        @pl.when(r > 0)
+        def _():
+            wait_recv(kv_z_in(zz))
+            start(kv_x(zz, x))
+
+        wait_recv(kv_x(zz, 1 - x))
+        state = key_step(zz * PAIR + 1, state)
+        return key_step(zz * PAIR, state)
+
+    running, _ = lax.fori_loop(
+        0, z + 1, key_round,
+        (jnp.zeros((group * tokens, HEAD_DIM), F32), jnp.zeros((group * tokens, 1), F32)),
+    )
+    scaled = running * lax.rsqrt(jnp.mean(running * running, axis=1, keepdims=True) + eps)
+    attended = jnp.concatenate(
+        [
+            scaled[g * tokens : (g + 1) * tokens] * gain[:, g * HEAD_DIM : (g + 1) * HEAD_DIM]
+            for g in range(group)
+        ],
+        axis=1,
+    ).astype(BF16)
+    for mm in range(members):
+        product = jnp.dot(
+            attended[mm * row_part : (mm + 1) * row_part], out_weight[...],
+            preferred_element_type=F32,
+        )
+        own_f32[mm] = product
+        own_cut[mm] = product.astype(BF16)
+
+    def pair_out(yy):
+        return remote(own_cut.at[yy * PAIR + 1 - c], pair_part.at[yy], "pc", yy, yy, tp=far_c)
+
+    for yy in range(PAIR):
+        pair_out(yy).start()
+
+    def weight_forward(e):
+        wait_recv(weight_z_in(toward(e)))
+        start(weight_x(toward(e), x))
+
+    for yy in range(PAIR):
+        pair_out(yy).wait_recv()
+    y_cut[...] = (own_f32[far_y] + pair_part[1 - y].astype(F32)).astype(BF16)
+    y_out = remote(y_cut, y_part, "py", 0, 0, tp=far_y)
+    y_out.start()
+    res_all[m] = residual[pl.ds(pl.multiple_of(m * row_part, row_part), row_part), :]
+    for d in range(1, members):
+        far = (m + d) % members
+        remote(res_all.at[far], res_all.at[far], "res", far, far, tp=far).wait_recv()
+    y_out.wait_recv()
+    hidden = jnp.concatenate([res_all[mm].astype(F32) for mm in range(members)], axis=1)
+    hidden = hidden + (own_f32[m] + pair_part[y].astype(F32) + y_part[...].astype(F32))
+    hidden = hidden.astype(BF16)
+    for mm in range(members):
+        hid_cut[mm] = hidden[:, mm * column_part : (mm + 1) * column_part]
+    widened = hidden.astype(F32)
+    inverse = lax.rsqrt(jnp.mean(widened * widened, axis=1, keepdims=True) + eps)
+    rows_all[z, m] = (widened * inverse * mlp_gain[...]).astype(BF16)
+
+    def rows_z(far):
+        return remote(rows_all.at[z, m], rows_all.at[z, m], "mz", far, z, sp=far * PAIR + x)
+
+    def rows_z_in(zz):
+        return remote(rows_all.at[zz, m], rows_all.at[zz, m], "mz", zz, zz, sp=far_x)
+
+    def rows_y(zz, mm):
+        return remote(rows_all.at[zz, mm], rows_all.at[zz, mm], "my", zz, zz, tp=far_y)
+
+    def rows_c(zz, yy, cc):
+        cell = rows_all.at[zz, yy * PAIR + cc]
+        return remote(cell, cell, "mc", zz * PAIR + yy, zz * PAIR + yy, tp=far_c)
+
+    def hid_out(far):
+        return remote(hid_cut.at[far], hid_all.at[m], "hid", far, m, tp=far)
+
+    for e in range(1, depth):
+        rows_z(toward(e)).start()
+    rows_y(z, m).start()
+    rows_c(z, y, c).start()
+    for d in range(1, members):
+        hid_out((m + d) % members).start()
+    hid_all[m] = hid_cut[m]
+    for e in range(1, depth):
+        weight_forward(e)
+        far = toward(e)
+        rows_z_in(far).wait_recv()
+        rows_y(far, m).start()
+        rows_c(far, y, c).start()
+    for e in range(depth):
+        far = toward(e)
+        rows_y(far, far_y).wait_recv()
+        rows_c(far, 1 - y, c).start()
+
+    for e in range(depth):
+        wait_recv(weight_x(toward(e), 1 - x))
+
+    def share_c(zz, yy):
+        return remote(
+            share.at[zz, yy * PAIR + 1 - c], pair_share.at[zz, yy], "rc",
+            zz * PAIR + yy, zz * PAIR + yy, tp=far_c,
+        )
+
+    def share_y(zz):
+        return remote(y_sum.at[zz], y_share.at[zz], "ry", zz, zz, tp=far_y)
+
+    def share_z(far):
+        return remote(z_sum.at[far], z_share.at[z], "rz", far, z, sp=far * PAIR + x)
+
+    def share_z_in(zz):
+        return remote(z_sum.at[zz], z_share.at[zz], "rz", zz, zz, sp=far_x)
+
+    def feed(k, carry):
+        zz = (z + 1 + k) % depth
+        for yy in range(PAIR):
+            rows_c(zz, yy, 1 - c).wait_recv()
+        rows = rows_all[zz].reshape(tokens, rows_all.shape[3])
+        lifted = jnp.dot(rows, up_all[...], preferred_element_type=F32)
+        activated = jnp.square(jnp.maximum(lifted, 0.0)).astype(BF16)
+        for mm in range(members):
+            share[zz, mm] = jnp.dot(
+                activated, down_all[mm], preferred_element_type=F32
+            ).astype(BF16)
+        for yy in range(PAIR):
+            share_c(zz, yy).start()
+        return carry
+
+    lax.fori_loop(0, depth, feed, 0)
+
+    def fold_pair(k, carry):
+        zz = (z + 1 + k) % depth
+        for yy in range(PAIR):
+            share_c(zz, yy).wait_recv()
+        y_sum[zz] = (
+            share[zz, far_y].astype(F32) + pair_share[zz, 1 - y].astype(F32)
+        ).astype(BF16)
+        share_y(zz).start()
+        return carry
+
+    lax.fori_loop(0, depth, fold_pair, 0)
+
+    def fold_y(k, carry):
+        zz = (z + 1 + k) % depth
+        share_y(zz).wait_recv()
+        total = (
+            share[zz, m].astype(F32) + pair_share[zz, y].astype(F32) + y_share[zz].astype(F32)
+        )
+
+        @pl.when(k < depth - 1)
+        def _():
+            z_sum[zz] = total.astype(BF16)
+            share_z(zz).start()
+
+        @pl.when(k == depth - 1)
+        def _():
+            own_total[...] = total
+
+        return carry
+
+    lax.fori_loop(0, depth, fold_y, 0)
+    for d in range(1, members):
+        far = (m + d) % members
+        remote(hid_all.at[far], hid_all.at[far], "hid", far, far, tp=far).wait_recv()
+    total = own_total[...]
+    for e in range(1, depth):
+        share_z_in(toward(e)).wait_recv()
+        total = total + z_share[toward(e)].astype(F32)
+    total = total + hid_all[...].astype(F32).reshape(tokens, column_part)
+    out[...] = total.astype(BF16)
+
+    def kv_sent(r, carry):
+        wait_send(kv_x(z - r, x))
+        return carry
+
+    lax.fori_loop(0, z + 1, kv_sent, 0)
+    for yy in range(PAIR):
+        pair_out(yy).wait_send()
+    y_out.wait_send()
+    for d in range(1, members):
+        residual_out((m + d) % members).wait_send()
+        hid_out((m + d) % members).wait_send()
+    for e in range(depth):
+        far = toward(e)
+        wait_send(weight_x(far, x))
+        rows_y(far, m).wait_send()
+        rows_c(far, y, c).wait_send()
+        rows_c(far, 1 - y, c).wait_send()
+        for yy in range(PAIR):
+            share_c(far, yy).wait_send()
+        share_y(far).wait_send()
+        if e:
+            wait_send(weight_z(far))
+            rows_z(far).wait_send()
+            share_z(far).wait_send()
+
+
+def whole_layer(depth, members, args):
+    (residual, queries, key_rows, value_rows, break_shift, head_gain, out_weight, mlp_gain,
+     up_weight, down_weight) = args
+    tokens, width = residual.shape[0], out_weight.shape[1]
+    positions = depth * PAIR
+    sub = up_weight.shape[1] // depth
+    column_part = residual.shape[1]
+    row_part = tokens // members
+    shift = jnp.broadcast_to(break_shift.astype(F32), (8, tokens))
+    _, sems = sem_bases(depth, members)
+    vmem = pl.BlockSpec(memory_space=pltpu.VMEM)
+    anywhere = pl.BlockSpec(memory_space=pl.ANY)
+    return pl.pallas_call(
+        functools.partial(layer_kernel, depth, members),
+        out_shape=jax.ShapeDtypeStruct(residual.shape, BF16),
+        in_specs=[vmem, anywhere, anywhere, anywhere, vmem, vmem, vmem, vmem, anywhere, anywhere],
+        out_specs=vmem,
+        scratch_shapes=[
+            pltpu.VMEM((positions, 2, tokens, HEAD_DIM), BF16),
+            pltpu.VMEM((positions, 8, tokens), F32),
+            pltpu.VMEM((width, sub), BF16),
+            pltpu.VMEM((depth, sub, column_part), BF16),
+            pltpu.VMEM((members, row_part, width), F32),
+            pltpu.VMEM((members, row_part, width), BF16),
+            pltpu.VMEM((PAIR, row_part, width), BF16),
+            pltpu.VMEM((row_part, width), BF16),
+            pltpu.VMEM((row_part, width), BF16),
+            pltpu.VMEM((members, row_part, column_part), BF16),
+            pltpu.VMEM((members, row_part, column_part), BF16),
+            pltpu.VMEM((members, row_part, column_part), BF16),
+            pltpu.VMEM((depth, members, row_part, width), BF16),
+            pltpu.VMEM((depth, members, tokens, column_part), BF16),
+            pltpu.VMEM((depth, PAIR, tokens, column_part), BF16),
+            pltpu.VMEM((depth, tokens, column_part), BF16),
+            pltpu.VMEM((depth, tokens, column_part), BF16),
+            pltpu.VMEM((depth, tokens, column_part), BF16),
+            pltpu.VMEM((depth, tokens, column_part), BF16),
+            pltpu.VMEM((tokens, column_part), F32),
+            pltpu.SemaphoreType.DMA((sems,)),
+            pltpu.SemaphoreType.DMA((sems,)),
+            pltpu.SemaphoreType.DMA((5,)),
+        ],
+        compiler_params=pltpu.CompilerParams(
+            collective_id=0, has_side_effects=True, vmem_limit_bytes=60 * 1024 * 1024
+        ),
+        name="layer",
+    )(
+        queries, key_rows, value_rows, shift, head_gain[None, :], residual, out_weight,
+        mlp_gain[None, :], up_weight, down_weight,
+    )
+
+
+def fits(depth, members, residual, key_rows, up_weight, down_weight):
+    return (
+        depth == members == PAIR * PAIR
+        and key_rows.shape[1] == HEAD_DIM
+        and residual.shape[0] % (128 * PAIR) == 0
+        and up_weight.shape[0] % 128 == 0
+        and down_weight.shape[1] * PAIR == residual.shape[1]
+        and up_weight.shape[0] == down_weight.shape[1]
+        and up_weight.shape[1] % (128 * depth) == 0
+    )
+
+
+def body(positions, members, *args):
+    depth = positions // PAIR
+    if fits(depth, members, args[0], args[2], args[8], args[9]):
+        return whole_layer(depth, members, args)
+    return gathered_body(*args)
+
+
 def solution(mesh):
     in_specs = (
         P("sp", "tp"),
@@ -124,4 +599,5 @@
         P("tp", "sp"),
     )
     out_specs = P("sp", "tp")
-    return jax.shard_map(body, mesh=mesh, in_specs=in_specs, out_specs=out_specs, check_vma=False)
+    return jax.shard_map(
+        functools.partial(body, mesh.shape["sp"], mesh.shape["tp"]), mesh=mesh, in_specs=in_specs, out_specs=out_specs, check_vma=False)

time: 313 us -> 136 us (0.43)
  Pallas kernels: 0 us -> 133 us
  blocking collectives: 127 us -> 0 us
  waiting for transfers between devices: 106 us -> 0 us
  matrix products: 25.2 us -> 0 us
  other arithmetic: 19.6 us -> 0.01 us
  local copies, waits for them, and re-layouts: 20.2 us -> 2.95 us
  between operations: 13.2 us -> 0.01 us
    pallas_call x0 -> x1, Pallas kernels: none -> 133 us  [whole_layer(): pl.pallas_call(functools.partial(layer_kernel, depth, members), out_shape...]
    all_gather x3 -> x0, blocking collectives: 86.4 us -> none  [the longest x1 33.3 us: body(): lax.all_gather(value_rows, 'sp', axis=0, tiled=True)]
    all_gather x2 -> x0, waiting for transfers between devices: 79.2 us -> none  [the longest x1 79.2 us: body(): lax.all_gather(down_weight, 'sp', axis=1, tiled=True)]
    psum x1 -> x0, blocking collectives: 40.5 us -> none  [body(): hidden_whole = lax.psum(partial_value, 'tp').astype(jnp.bfloat16)]
    dot_general x4 -> x0, matrix products: 25.2 us -> none  [the longest x1 11.6 us: body(): jnp.dot(activated, lax.all_gather(down_weight, 'sp', axis=1, tiled=True),...]
    reduce_scatter x1 -> x0, waiting for transfers between devices: 25 us -> none  [body(): lax.psum_scatter(expanded.astype(jnp.bfloat16), 'tp', scatter_dimension=1...]
    another operation x6 -> x0, local copies, waits for them, and re-layouts: 14.2 us -> none
    another operation x2 -> x0, other arithmetic: 10.9 us -> none
  transfers between devices with their start and end apart: 3 -> 0, of which waited for: 2 -> 0; matrix products, arithmetic and copies ran while one was open for 16% -> 0% of each run, Pallas kernels for 0% -> 0%
where the time goes in v1:
time: 136 us
  Pallas kernels  133 us (98%)
  local copies, waits for them, and re-layouts  2.95 us (2%)
    pallas_call x1, Pallas kernels, whole_layer(): pl.pallas_call(functools.partial(layer_kernel, depth, members), out_shape...  133 us

profile of v1, /device:TPU:8, one launch (start us, length us, event | category | flops | bytes accessed | tf_op | source)
XLA Modules:
  0.0 135.9 jit_solution(15193502231995743490)
XLA Ops:
  0.0 0.0 copy-start
  0.0 0.7 copy-done
  0.7 0.6 broadcast_in_dim.18.shift
  1.3 132.9 %layer.1 = bf16[256,512]{1,0:T(8,128)(2,1)} custom-call(bf16[256,256]{1,0:T(8,128)(2,1)} %queries.1, bf16[256,128]{1,0:T(8,128)(2,1)} %keys.1, bf16[256,128]{1,0:T(8,128)(2,1)} %values.1, f32[8,256]{1,0:T(8,128)} %broadcast_in_dim.18.shift, f32[1,256]{1,0:T(1,128)} %bitcast.5, bf16[256,512]{1,0:T(8,128)(2,1)} %residual.1, bf16[256,2048]{1,0:T(8,128)(2,1)} %out_weight.1, ...), custom_call_target="tpu_custom_call" | custom-call | tf_op jit(solution)/shard_map/layer/pallas_call | solution.py:529
  134.2 1.7 %copy.12 = bf16[256,512]{1,0:T(8,128)(2,1)} copy(bf16[256,512]{1,0:T(8,128)(2,1)} %layer.1) | data formatting | bytes 524288
  (1 shorter events, 0.0 us)
Async XLA Ops:
  0.0 0.7 copy-start

commit v2 on v1

--- a/solution.py
+++ b/solution.py
@@ -123,7 +123,7 @@
         ("kvz", depth), ("kvx", depth), ("shz", depth), ("shx", depth),
         ("upz", depth), ("dnz", depth), ("upx", depth), ("dnx", depth),
         ("res", members), ("hid", members), ("pc", PAIR), ("py", 1),
-        ("mz", depth), ("my", depth), ("mc", PAIR * depth),
+        ("mz", PAIR * depth), ("my", depth), ("mc", PAIR * depth),
         ("rc", PAIR * depth), ("ry", depth), ("rz", depth),
     )
     base, total = {}, 0
@@ -137,7 +137,7 @@
     depth, members, queries, keys, values, shift, gain, residual, out_weight, mlp_gain, up, down,
     out, kv_all, shift_all, up_all, down_all, own_f32, own_cut, pair_part, y_cut, y_part,
     res_all, hid_cut, hid_all, rows_all, share, pair_share, y_sum, y_share, z_sum, z_share,
-    own_total, send_sem, recv_sem, local_sem,
+    own_total, activated, send_sem, recv_sem, local_sem,
 ):
     base, _ = sem_bases(depth, members)
     me, m = lax.axis_index("sp"), lax.axis_index("tp")
@@ -157,6 +157,10 @@
             bit *= 2
         return far
 
+    inner = ((z + 1) // 2) % 2
+    near = [toward(1), toward(2) + inner * (toward(3) - toward(2))]
+    near.append(toward(3) + inner * (toward(2) - toward(3)))
+
     def remote(src, dst, name, send, recv, sp=me, tp=m):
         return pltpu.make_async_remote_copy(
             src_ref=src, dst_ref=dst, send_sem=send_sem.at[base[name] + send],
@@ -268,21 +272,25 @@
     start(kv_x(z, x))
     for d in range(1, members):
         residual_out((m + d) % members).start()
-    for d in range(1, depth):
-        @pl.when(z - d >= 0)
-        def _():
-            start(weight_z(z - d))
+    for far in near:
+        @pl.when(far < z)
+        def _():
+            start(weight_z(far))
     for copy in own_weights:
         copy.wait()
-    start(weight_x(z, x))
+
+    @pl.when(z == 0)
+    def _():
+        start(weight_x(z, x))
+
     for d in range(1, depth):
         @pl.when(z + d < depth)
         def _():
             wait_send(kv_z(z + d))
-    for d in range(1, depth):
-        @pl.when(z + d < depth)
-        def _():
-            start(weight_z(z + d))
+    for far in near:
+        @pl.when(far > z)
+        def _():
+            start(weight_z(far))
 
     group = queries.shape[1] // HEAD_DIM
     stacked = jnp.concatenate(
@@ -317,13 +325,26 @@
         running = running + jnp.dot(stick, kv_all[at, 1], preferred_element_type=F32)
         return running, after + jnp.sum(broken, axis=1, keepdims=True)
 
+    def weight_forward(far):
+        for arrived, onward in zip(weight_z_in(far), weight_x(far, x)):
+            arrived.wait_recv()
+            onward.start()
+
     def key_round(r, state):
         zz = z - r
 
+        @pl.when(r == 3)
+        def _():
+            weight_forward(near[0])
+
         @pl.when(r > 0)
         def _():
             wait_recv(kv_z_in(zz))
             start(kv_x(zz, x))
+
+        @pl.when(jnp.logical_and(r > 0, r == jnp.minimum(z, 2)))
+        def _():
+            start(weight_x(z, x))
 
         wait_recv(kv_x(zz, 1 - x))
         state = key_step(zz * PAIR + 1, state)
@@ -355,9 +376,9 @@
     for yy in range(PAIR):
         pair_out(yy).start()
 
-    def weight_forward(e):
-        wait_recv(weight_z_in(toward(e)))
-        start(weight_x(toward(e), x))
+    @pl.when(z < 3)
+    def _():
+        weight_forward(near[0])
 
     for yy in range(PAIR):
         pair_out(yy).wait_recv()
@@ -378,8 +399,14 @@
     inverse = lax.rsqrt(jnp.mean(widened * widened, axis=1, keepdims=True) + eps)
     rows_all[z, m] = (widened * inverse * mlp_gain[...]).astype(BF16)
 
-    def rows_z(far):
-        return remote(rows_all.at[z, m], rows_all.at[z, m], "mz", far, z, sp=far * PAIR + x)
+    def rows_hop(zz, step):
+        return remote(
+            rows_all.at[zz, m], rows_all.at[zz, m], "mz",
+            zz if step > 0 else depth + zz, zz, sp=(z + step) * PAIR + x,
+        )
+
+    def inside(zz):
+        return jnp.logical_and(zz >= 0, zz < depth)
 
     def rows_z_in(zz):
         return remote(rows_all.at[zz, m], rows_all.at[zz, m], "mz", zz, zz, sp=far_x)
@@ -394,26 +421,38 @@
     def hid_out(far):
         return remote(hid_cut.at[far], hid_all.at[m], "hid", far, m, tp=far)
 
-    for e in range(1, depth):
-        rows_z(toward(e)).start()
+    for step in (1, -1):
+        @pl.when(inside(z + step))
+        def _():
+            rows_hop(z, step).start()
     rows_y(z, m).start()
     rows_c(z, y, c).start()
     for d in range(1, members):
         hid_out((m + d) % members).start()
     hid_all[m] = hid_cut[m]
-    for e in range(1, depth):
-        weight_forward(e)
-        far = toward(e)
-        rows_z_in(far).wait_recv()
-        rows_y(far, m).start()
-        rows_c(far, y, c).start()
+    weight_forward(near[1])
+    weight_forward(near[2])
+    for d in range(1, depth):
+        for step in (1, -1):
+            far = z - step * d
+
+            @pl.when(inside(far))
+            def _():
+                rows_z_in(far).wait_recv()
+
+                @pl.when(inside(z + step))
+                def _():
+                    rows_hop(far, step).start()
+
+                rows_y(far, m).start()
+                rows_c(far, y, c).start()
     for e in range(depth):
         far = toward(e)
         rows_y(far, far_y).wait_recv()
         rows_c(far, 1 - y, c).start()
 
     for e in range(depth):
-        wait_recv(weight_x(toward(e), 1 - x))
+        weight_x(toward(e), 1 - x)[0].wait_recv()
 
     def share_c(zz, yy):
         return remote(
@@ -430,24 +469,35 @@
     def share_z_in(zz):
         return remote(z_sum.at[zz], z_share.at[zz], "rz", zz, zz, sp=far_x)
 
-    def feed(k, carry):
+    def lift(k, carry):
         zz = (z + 1 + k) % depth
         for yy in range(PAIR):
             rows_c(zz, yy, 1 - c).wait_recv()
         rows = rows_all[zz].reshape(tokens, rows_all.shape[3])
         lifted = jnp.dot(rows, up_all[...], preferred_element_type=F32)
-        activated = jnp.square(jnp.maximum(lifted, 0.0)).astype(BF16)
+        activated[zz] = jnp.square(jnp.maximum(lifted, 0.0)).astype(BF16)
+        return carry
+
+    lax.fori_loop(0, depth, lift, 0)
+    for e in range(depth):
+        weight_x(toward(e), 1 - x)[1].wait_recv()
+
+    def feed(k, carry):
+        zz = (z + 1 + k) % depth
         for mm in range(members):
             share[zz, mm] = jnp.dot(
-                activated, down_all[mm], preferred_element_type=F32
+                activated[zz], down_all[mm], preferred_element_type=F32
             ).astype(BF16)
         for yy in range(PAIR):
             share_c(zz, yy).start()
+
+        @pl.when(k > 0)
+        def _():
+            fold_pair(k - 1)
+
         return carry
 
-    lax.fori_loop(0, depth, feed, 0)
-
-    def fold_pair(k, carry):
+    def fold_pair(k):
         zz = (z + 1 + k) % depth
         for yy in range(PAIR):
             share_c(zz, yy).wait_recv()
@@ -455,9 +505,9 @@
             share[zz, far_y].astype(F32) + pair_share[zz, 1 - y].astype(F32)
         ).astype(BF16)
         share_y(zz).start()
-        return carry
-
-    lax.fori_loop(0, depth, fold_pair, 0)
+
+    lax.fori_loop(0, depth, feed, 0)
+    fold_pair(depth - 1)
 
     def fold_y(k, carry):
         zz = (z + 1 + k) % depth
@@ -493,6 +543,17 @@
         return carry
 
     lax.fori_loop(0, z + 1, kv_sent, 0)
+    for d in range(depth):
+        for step in (1, -1) if d else (1,):
+            far = z - step * d
+
+            @pl.when(inside(far))
+            def _():
+                for hop in (step,) if d else (1, -1):
+                    @pl.when(inside(z + hop))
+                    def _():
+                        rows_hop(far, hop).wait_send()
+
     for yy in range(PAIR):
         pair_out(yy).wait_send()
     y_out.wait_send()
@@ -510,7 +571,6 @@
         share_y(far).wait_send()
         if e:
             wait_send(weight_z(far))
-            rows_z(far).wait_send()
             share_z(far).wait_send()
 
 
@@ -552,6 +612,7 @@
             pltpu.VMEM((depth, tokens, column_part), BF16),
             pltpu.VMEM((depth, tokens, column_part), BF16),
             pltpu.VMEM((tokens, column_part), F32),
+            pltpu.VMEM((depth, tokens, sub), BF16),
             pltpu.SemaphoreType.DMA((sems,)),
             pltpu.SemaphoreType.DMA((sems,)),
             pltpu.SemaphoreType.DMA((5,)),

time: 136 us -> 130 us (0.956)
  Pallas kernels: 133 us -> 127 us
    pallas_call x1, Pallas kernels: 133 us -> 127 us  [whole_layer(): pl.pallas_call(functools.partial(layer_kernel, depth, members), out_shape...]
where the time goes in v2:
time: 130 us
  Pallas kernels  127 us (98%)
  local copies, waits for them, and re-layouts  2.95 us (2%)
    pallas_call x1, Pallas kernels, whole_layer(): pl.pallas_call(functools.partial(layer_kernel, depth, members), out_shape...  127 us

profile of v2, /device:TPU:8, one launch (start us, length us, event | category | flops | bytes accessed | tf_op | source)
XLA Modules:
  0.0 130.0 jit_solution(10440795924350826035)
XLA Ops:
  0.0 0.0 copy-start
  0.0 0.7 copy-done
  0.7 0.6 broadcast_in_dim.18.shift
  1.3 127.0 %layer.1 = bf16[256,512]{1,0:T(8,128)(2,1)} custom-call(bf16[256,256]{1,0:T(8,128)(2,1)} %queries.1, bf16[256,128]{1,0:T(8,128)(2,1)} %keys.1, bf16[256,128]{1,0:T(8,128)(2,1)} %values.1, f32[8,256]{1,0:T(8,128)} %broadcast_in_dim.18.shift, f32[1,256]{1,0:T(1,128)} %bitcast.5, bf16[256,512]{1,0:T(8,128)(2,1)} %residual.1, bf16[256,2048]{1,0:T(8,128)(2,1)} %out_weight.1, ...), custom_call_target="tpu_custom_call" | custom-call | tf_op jit(solution)/shard_map/layer/pallas_call | solution.py:589
  128.3 1.7 %copy.12 = bf16[256,512]{1,0:T(8,128)(2,1)} copy(bf16[256,512]{1,0:T(8,128)(2,1)} %layer.1) | data formatting | bytes 524288
  (1 shorter events, 0.0 us)
Async XLA Ops:
  0.0 0.7 copy-start
